TPU v7x, 32 devices: a whole 2x2x4 slice. The times are simulated.
32 devices in a mesh: ep: 4 (over y, x), tp: 8 (over z, core).
Axes of the slice: x: 2, y: 2, z: 4, core: 2. Of those that a mesh axis runs over, the one named last changes fastest.
Arguments:
- queries: bfloat16 [4096, 1024], P('ep', 'tp'), may hold values from -6 to 6
- keys: bfloat16 [4096, 256], P('ep'), may hold values from -6 to 6, as said below
- values: bfloat16 [4096, 256], P('ep'), may hold values from -6 to 6
- slopes: float32 [16], P('tp'), may hold values from 0.002 to 0.08
- sinks: float32 [16], P('tp'), may hold values from 2 to 6
- out_weight: bfloat16 [1024, 2048], P('tp'), may hold values from -0.1875 to 0.1875
- mix_gain: float32 [2048], replicated, may hold values from 0.1 to 1.9
- moe_input: bfloat16 [4096, 2048], P(('ep', 'tp')), may hold values from -6 to 6
- in_gain: float32 [2048], replicated, may hold values from 0.1 to 1.9
- out_gain: float32 [2048], replicated, may hold values from 0.1 to 1.9
- group_router: bfloat16 [2048, 4], replicated, may hold values from -0.125 to 0.125
- expert_router: bfloat16 [2048, 4], replicated, may hold values from -0.125 to 0.125
- routes: int32 [4096, 2], P(('ep', 'tp')), may hold values from 0 to 3, all different within a row; in each aligned block of 128 rows (0 to 127, 128 to 255, ...) at most 96 rows name the same one
- gate_weight: bfloat16 [4, 2048, 1024], P('ep', None, 'tp'), may hold values from -0.125 to 0.125
- up_weight: bfloat16 [4, 2048, 1024], P('ep', None, 'tp'), may hold values from -0.125 to 0.125
- down_weight: bfloat16 [4, 2048, 1024], P('ep', None, 'tp'), may hold values from -0.1875 to 0.1875
Outputs:
- mixer_output: bfloat16 [4096, 2048], P(('ep', 'tp'))
- moe_output: bfloat16 [4096, 2048], P(('ep', 'tp'))
Inputs may be any that keep to these rules, and one draw needn't show every extreme that they name: `keys`: keys share one value range with the queries. `routes`: A token names 2 different experts. Among the rows of one device no expert is named more than 96 times, a bound that some block reaches in every draw.
All inputs are finite; a program needn't handle non-finite values.
Results may differ from a plain program's by a relative error of at most 0.018.
Values may be sent and summed in bfloat16 or wider, within the bound.
No kernel may reach another device: no remote copies, remote signals or barrier semaphores. Data moves between devices by JAX's collectives and lax.ppermute only.
A program may use at most 128 MiB of HBM per device.

v0:
```python
import math
import jax
import jax.numpy as jnp
from jax import lax
from jax.sharding import PartitionSpec as P

HEADS = 16
HD = 64
KV_HEADS = 4
WINDOW = 128
eps = 1e-06


def shifted(block, axis, distance):
    devices = range(lax.axis_size(axis))
    route = [(i - distance, i) for i in devices if i - distance in devices]
    return lax.ppermute(block, axis, route)


def scale_rows(matrix, gain):
    mean_square = jnp.mean(matrix * matrix, axis=-1, keepdims=True)
    return matrix * lax.rsqrt(mean_square + eps) * gain


def per_device(
    queries,
    keys,
    values,
    slopes,
    sinks,
    out_weight,
    mix_gain,
    moe_input,
    in_gain,
    out_gain,
    group_router,
    expert_router,
    routes,
    gate_weight,
    up_weight,
    down_weight,
):
    rows_group = queries.shape[0]
    local_heads = slopes.shape[0]
    per_kv = HEADS // KV_HEADS
    kv_index = lax.axis_index("tp") * local_heads // per_kv
    own_keys = lax.dynamic_slice_in_dim(keys, kv_index * HD, HD, 1)
    own_values = lax.dynamic_slice_in_dim(values, kv_index * HD, HD, 1)
    rim_keys, rim_values = shifted(
        (own_keys[rows_group - WINDOW :], own_values[rows_group - WINDOW :]), "ep", 1
    )
    blocks = rows_group // WINDOW
    key_blocks = own_keys.reshape(blocks, WINDOW, HD)
    value_blocks = own_values.reshape(blocks, WINDOW, HD)
    key_span = jnp.concatenate(
        [jnp.concatenate([rim_keys[None], key_blocks[:-1]], axis=0), key_blocks], axis=1
    )
    value_span = jnp.concatenate(
        [jnp.concatenate([rim_values[None], value_blocks[:-1]], axis=0), value_blocks], axis=1
    )
    query_blocks = queries.reshape(blocks, WINDOW, local_heads, HD)
    scores = jnp.einsum(
        "nqhd,nsd->nhqs", query_blocks, key_span, preferred_element_type=jnp.float32
    ) * (1.0 / math.sqrt(HD))
    query_index = jnp.arange(WINDOW, dtype=jnp.int32)[:, None]
    key_index = jnp.arange(2 * WINDOW, dtype=jnp.int32)[None, :]
    distance = query_index + WINDOW - key_index
    key_position = (
        lax.axis_index("ep") * rows_group
        + jnp.arange(blocks, dtype=jnp.int32)[:, None, None] * WINDOW
        + key_index[None]
        - WINDOW
    )
    valid = ((distance >= 0) & (distance < WINDOW))[None] & (key_position >= 0)
    scores = scores - slopes[None, :, None, None] * distance.astype(jnp.float32)[None, None]
    scores = jnp.where(valid[:, None], scores, -jnp.inf)
    sink = sinks[None, :, None, None]
    top = jnp.maximum(jnp.max(scores, axis=-1, keepdims=True), sink)
    weights = jnp.exp(scores - top)
    denom = jnp.sum(weights, axis=-1, keepdims=True) + jnp.exp(sink - top)
    probs = (weights / denom).astype(jnp.bfloat16)
    attention = jnp.einsum("nhqs,nsd->nqhd", probs, value_span, preferred_element_type=jnp.float32)
    attention = attention.astype(jnp.bfloat16).reshape(rows_group, local_heads * HD)
    own_rows = moe_input.shape[0]
    projected = lax.psum_scatter(
        jnp.dot(attention, out_weight, preferred_element_type=jnp.float32).astype(jnp.bfloat16),
        "tp",
        scatter_dimension=0,
        tiled=True,
    ).astype(jnp.float32)
    mixer_output = scale_rows(projected, mix_gain).astype(jnp.bfloat16)
    normed = scale_rows(moe_input.astype(jnp.float32), in_gain).astype(jnp.bfloat16)
    group_logits = jnp.dot(normed, group_router, preferred_element_type=jnp.float32)
    expert_logits = jnp.dot(normed, expert_router, preferred_element_type=jnp.float32)
    experts = expert_router.shape[1]
    groups = group_router.shape[1]
    per_group = experts // groups
    visits = routes.shape[1]
    expert_match = routes[:, :, None] == jnp.arange(experts, dtype=jnp.int32)[None, None, :]
    picked_logits = jnp.sum(jnp.where(expert_match, expert_logits[:, None, :], 0.0), axis=-1)
    group_prob = jax.nn.softmax(group_logits, axis=-1)
    group_match = (routes // per_group)[:, :, None] == jnp.arange(groups, dtype=jnp.int32)[
        None, None, :
    ]
    picked_group = jnp.sum(jnp.where(group_match, group_prob[:, None, :], 0.0), axis=-1)
    route_weight = picked_group * jax.nn.softmax(picked_logits, axis=-1)
    capacity = max(2, 3 * own_rows * visits // (2 * experts))
    match_int = expert_match.astype(jnp.int32).reshape(own_rows * visits, experts)
    before = jnp.cumsum(match_int, axis=0) - match_int
    slot = jnp.sum(before * match_int, axis=-1)
    position = (routes.reshape(-1) * capacity + slot).reshape(own_rows, visits)
    slot_ids = jnp.arange(experts * capacity, dtype=jnp.int32)
    placement = jnp.any(position[None, :, :] == slot_ids[:, None, None], axis=-1).astype(
        jnp.bfloat16
    )
    outgoing = jnp.dot(placement, normed, preferred_element_type=jnp.float32).astype(jnp.bfloat16)
    local_experts = gate_weight.shape[0]
    outgoing = outgoing.reshape(lax.axis_size("ep"), local_experts, capacity, normed.shape[1])
    arrived = lax.all_to_all(outgoing, "ep", split_axis=0, concat_axis=0, tiled=True)
    gate_piece = lax.all_gather(gate_weight, "tp", axis=2, tiled=True)
    up_piece = lax.all_gather(up_weight, "tp", axis=2, tiled=True)
    down_piece = lax.all_gather(down_weight, "tp", axis=2, tiled=True)
    gate = jnp.einsum("sxcd,xdf->sxcf", arrived, gate_piece, preferred_element_type=jnp.float32)
    up = jnp.einsum("sxcd,xdf->sxcf", arrived, up_piece, preferred_element_type=jnp.float32)
    hidden = (jax.nn.silu(gate) * up).astype(jnp.bfloat16)
    results = jnp.einsum("sxcf,xdf->sxcd", hidden, down_piece, preferred_element_type=jnp.float32)
    returned = lax.all_to_all(
        results.astype(jnp.bfloat16), "ep", split_axis=0, concat_axis=0, tiled=True
    )
    flat_back = returned.reshape(experts * capacity, returned.shape[3])
    picked_rows = jnp.take(flat_back, position.reshape(-1), axis=0).reshape(
        own_rows, visits, flat_back.shape[1]
    )
    moe = jnp.sum(route_weight[:, :, None] * picked_rows.astype(jnp.float32), axis=1)
    moe_output = scale_rows(moe, out_gain).astype(jnp.bfloat16)
    return (mixer_output, moe_output)


def solution(mesh):
    return jax.shard_map(
        per_device,
        mesh=mesh,
        in_specs=(
            P("ep", "tp"),
            P("ep", None),
            P("ep", None),
            P("tp"),
            P("tp"),
            P("tp", None),
            P(),
            P(("ep", "tp"), None),
            P(),
            P(),
            P(),
            P(),
            P(("ep", "tp"), None),
            P("ep", None, "tp"),
            P("ep", None, "tp"),
            P("ep", None, "tp"),
        ),
        out_specs=(P(("ep", "tp"), None), P(("ep", "tp"), None)),
        check_vma=False,
    )
```

profile of v0, /device:TPU:0, one launch (start us, length us, event | category | flops | bytes accessed | tf_op | source)
XLA Modules:
  0.0 222.8 jit_solution(3067624268574023449)
XLA Ops:
  7.2 0.7 all-gather.6.cloned.1.call-update
  8.0 0.7 all-gather.4.cloned.1.call-update
  8.7 0.7 all-gather.8.cloned.1.call-update
  9.5 1.2 constant_dynamic-slice_fusion
  10.9 4.9 %collective-permute-start.1 = (bf16[128,64]{0,1:T(8,128)(2,1)S(1)}, bf16[128,64]{0,1:T(8,128)(2,1)S(1)}, u32[]{:S(2)}, u32[]{:S(2)}) collective-permute-start(bf16[128,64]{0,1:T(8,128)(2,1)S(1)} %slice.36), channel_id=1, source_target_pairs={{0,8},{8,16},{16,24},{1,9},{9,17},{17,25},{2,10},{10,18},{18,26},{... | collective-permute-start | bytes 49160 | tf_op jit(solution)/shard_map/ppermute | solution.py:17
  15.9 3.4 %collective-permute-start = (bf16[128,64]{0,1:T(8,128)(2,1)S(1)}, bf16[128,64]{0,1:T(8,128)(2,1)S(1)}, u32[]{:S(2)}, u32[]{:S(2)}) collective-permute-start(bf16[128,64]{0,1:T(8,128)(2,1)S(1)} %slice.34), channel_id=1, source_target_pairs={{0,8},{8,16},{16,24},{1,9},{9,17},{17,25},{2,10},{10,18},{18,26},{... | collective-permute-start | bytes 49160 | tf_op jit(solution)/shard_map/ppermute | solution.py:17
  19.6 0.3 broadcast_and_fusion
  20.1 0.2 reshape.313
  20.3 0.6 fusion.73
  21.1 0.3 fusion.13
  21.5 0.5 fusion.20
  22.2 3.2 %convolution_convert_fusion = bf16[1024,2048]{1,0:T(8,128)(2,1)} fusion(bf16[128,2048]{1,0:T(8,128)(2,1)S(1)} %copy-done, bf16[16,8,8,128]{3,2,1,0:T(8,128)(2,1)S(1)} %bitcast.155), kind=kOutput, calls=%fused_computation.7 | convolution fusion | flops 538968064 | bytes 4980736 | tf_op jit(solution)/shard_map/dot_general | solution.py:86
  25.4 0.6 copy-done.3
  26.5 1.2 reduce-window.6
  28.6 1.8 convolution_convert_fusion.1
  30.4 3.9 %all-to-all-start = ((bf16[4,1,96,2048]{3,2,1,0:T(8,128)(2,1)}), bf16[4,1,96,2048]{3,2,1,0:T(8,128)(2,1)S(1)}, u32[]{:S(2)}, u32[]{:S(2)}) async-start(bf16[4,1,96,2048]{3,2,1,0:T(8,128)(2,1)} %bitcast.11), calls=%async_computation.1 | async-start | bytes 3145728 | tf_op jit(solution)/shard_map/all_to_all | solution.py:119
  34.3 0.3 fusion.74
  34.7 0.3 fusion.68
  35.5 17.6 %all-to-all-done = bf16[4,1,96,2048]{3,2,1,0:T(8,128)(2,1)S(1)} async-done(((bf16[4,1,96,2048]{3,2,1,0:T(8,128)(2,1)}), bf16[4,1,96,2048]{3,2,1,0:T(8,128)(2,1)S(1)}, u32[]{:S(2)}, u32[]{:S(2)}) %all-to-all-start) | async-done | bytes 1572896 | tf_op jit(solution)/shard_map/all_to_all | solution.py:119
  53.1 7.1 %all-gather.6.cloned.1.call-done = bf16[1,2048,1024]{2,1,0:T(8,128)(2,1)} async-done(((bf16[1,2048,128]{2,1,0:T(8,128)(2,1)}), bf16[1,2048,1024]{2,1,0:T(8,128)(2,1)}) %all-gather.6.cloned.1.call-update) | async-done | bytes 4194320 | tf_op jit(solution)/shard_map/all_gather | solution.py:121
  60.2 5.1 %fusion.2 = f32[4,96,1024]{2,1,0:T(8,128)} fusion(bf16[1,2048,1024]{2,1,0:T(8,128)(2,1)} %all-gather.6.cloned.1.call-done, bf16[4,1,96,2048]{3,2,1,0:T(8,128)(2,1)S(1)} %all-to-all-done), kind=kOutput, calls=%fused_computation.3 | convolution fusion | flops 1610612736 | bytes 7340032 | tf_op jit(solution)/shard_map/sxcd,xdf->sxcf/dot_general | solution.py:124
  65.3 42.5 %all-gather.4.cloned.1.call-done = bf16[1,2048,1024]{2,1,0:T(8,128)(2,1)} async-done(((bf16[1,2048,128]{2,1,0:T(8,128)(2,1)}), bf16[1,2048,1024]{2,1,0:T(8,128)(2,1)}) %all-gather.4.cloned.1.call-update) | async-done | bytes 4194320 | tf_op jit(solution)/shard_map/all_gather | solution.py:120
  107.8 47.6 %all-gather.8.cloned.1.call-done = bf16[1,2048,1024]{2,1,0:T(8,128)(2,1)} async-done(((bf16[1,2048,128]{2,1,0:T(8,128)(2,1)}), bf16[1,2048,1024]{2,1,0:T(8,128)(2,1)}) %all-gather.8.cloned.1.call-update) | async-done | bytes 4194320 | tf_op jit(solution)/shard_map/all_gather | solution.py:122
  155.4 8.6 %fusion.9 = bf16[4,1,96,2048]{3,2,1,0:T(8,128)(2,1)} fusion(bf16[1,2048,1024]{2,1,0:T(8,128)(2,1)} %all-gather.8.cloned.1.call-done, f32[4,96,1024]{2,1,0:T(8,128)} %fusion.2, bf16[1,2048,1024]{2,1,0:T(8,128)(2,1)} %all-gather.4.cloned.1.call-done, bf16[4,1,96,2048]{3,2,1,0:T(8,128)(2,1)S(1)} %all-to-all-done), kind=kOutput, calls=%fused_computation.10 | convolution fusion | flops 3224371200 | bytes 13107200 | tf_op jit(solution)/shard_map/sxcf,xdf->sxcd/dot_general | solution.py:126
  164.1 3.9 %all-to-all-start.1 = ((bf16[4,1,96,2048]{3,2,1,0:T(8,128)(2,1)}), bf16[4,1,96,2048]{3,2,1,0:T(8,128)(2,1)S(1)}, u32[]{:S(2)}, u32[]{:S(2)}) async-start(bf16[4,1,96,2048]{3,2,1,0:T(8,128)(2,1)} %fusion.9), calls=%async_computation.2 | async-start | bytes 3145728 | tf_op jit(solution)/shard_map/all_to_all | solution.py:127
  168.1 37.6 %reduce-scatter.2.cloned.1.call-done = bf16[128,2048]{1,0:T(8,128)(2,1)} async-done(((bf16[1024,2048]{1,0:T(8,128)(2,1)}), bf16[128,2048]{1,0:T(8,128)(2,1)}) %reduce-scatter.2.cloned.1.call-update) | async-done | bytes 524304 | tf_op jit(solution)/shard_map/reduce_scatter | solution.py:85
  205.7 1.2 fusion.30
  207.0 2.0 fusion.32
  209.0 1.4 gather_fusion
  210.4 0.7 gather.7
  211.1 4.1 %multiply_reduce_fusion = f32[128,2048]{1,0:T(8,128)S(1)} fusion(bf16[128,2,2048]{2,1,0:T(2,128)(2,1)S(1)} %gather.7, pred[128,2]{1,0:T(8,128)(4,1)S(1)} %copy.102, f32[128,2]{1,0:T(8,128)S(1)} %copy.96), kind=kLoop, calls=%fused_computation.13 | loop fusion | flops 1835008 | bytes 2098432 | tf_op jit(solution)/shard_map/reduce_sum | solution.py:134
  215.3 1.0 multiply_convert_fusion
  (79 shorter events, 3.2 us)
Async XLA Ops:
  7.2 15.0 %copy-start = (bf16[128,2048]{1,0:T(8,128)(2,1)S(1)}, bf16[128,2048]{1,0:T(8,128)(2,1)}, u32[]{:S(2)}) copy-start(bf16[128,2048]{1,0:T(8,128)(2,1)} %param.21) | copy-start | bytes 1572868
  7.2 53.0 %all-gather.6.cloned.1.call-start = ((), (), s32[]{:S(2)}) async-start(), calls=%async_computation.5 | async-start | bytes 4718592 | tf_op jit(solution)/shard_map/all_gather | solution.py:121
  7.9 12.0 %copy-start.8 = (f32[2]{0:T(128)S(1)}, f32[2]{0:T(128)}, u32[]{:S(2)}) copy-start(f32[2]{0:T(128)} %param.19) | copy-start | bytes 28
  7.9 99.9 %all-gather.4.cloned.1.call-start = ((), (), s32[]{:S(2)}) async-start(), calls=%async_computation.4 | async-start | bytes 4718592 | tf_op jit(solution)/shard_map/all_gather | solution.py:120
  8.7 11.4 %copy-start.2 = (bf16[1024,128]{1,0:T(8,128)(2,1)S(1)}, bf16[1024,128]{1,0:T(8,128)(2,1)}, u32[]{:S(2)}) copy-start(bf16[1024,128]{1,0:T(8,128)(2,1)} %param.16) | copy-start | bytes 786436
  8.7 146.7 %all-gather.8.cloned.1.call-start = ((), (), s32[]{:S(2)}) async-start(), calls=%async_computation.6 | async-start | bytes 4718592 | tf_op jit(solution)/shard_map/all_gather | solution.py:122
  9.4 196.3 %reduce-scatter.2.cloned.1.call-start = ((), (), s32[]{:S(2)}) async-start(), calls=%async_computation.3 | async-start | bytes 4718592 | tf_op jit(solution)/shard_map/reduce_scatter | solution.py:85
  10.9 9.4 %collective-permute-start.1 = (bf16[128,64]{0,1:T(8,128)(2,1)S(1)}, bf16[128,64]{0,1:T(8,128)(2,1)S(1)}, u32[]{:S(2)}, u32[]{:S(2)}) collective-permute-start(bf16[128,64]{0,1:T(8,128)(2,1)S(1)} %slice.36), channel_id=1, source_target_pairs={{0,8},{8,16},{16,24},{1,9},{9,17},{17,25},{2,10},{10,18},{18,26},{... | collective-permute-start | bytes 49160 | tf_op jit(solution)/shard_map/ppermute | solution.py:17
  15.9 5.6 %collective-permute-start = (bf16[128,64]{0,1:T(8,128)(2,1)S(1)}, bf16[128,64]{0,1:T(8,128)(2,1)S(1)}, u32[]{:S(2)}, u32[]{:S(2)}) collective-permute-start(bf16[128,64]{0,1:T(8,128)(2,1)S(1)} %slice.34), channel_id=1, source_target_pairs={{0,8},{8,16},{16,24},{1,9},{9,17},{17,25},{2,10},{10,18},{18,26},{... | collective-permute-start | bytes 49160 | tf_op jit(solution)/shard_map/ppermute | solution.py:17
  20.3 0.7 copy-start.7
  25.4 0.7 copy-start.3
  25.4 3.0 %copy-start.1 = (bf16[128,2048]{1,0:T(8,128)(2,1)S(1)}, bf16[128,2048]{1,0:T(8,128)(2,1)}, u32[]{:S(2)}) copy-start(bf16[128,2048]{1,0:T(8,128)(2,1)} %param.23) | copy-start | bytes 1572868
  25.4 3.2 %copy-start.4 = (f32[2048]{0:T(1024)S(1)}, f32[2048]{0:T(1024)}, u32[]{:S(2)}) copy-start(f32[2048]{0:T(1024)} %param.24) | copy-start | bytes 24580
  30.4 3.9 %copy-start.9 = (bf16[2048,4]{0,1:T(4,128)(2,1)S(1)}, bf16[2048,4]{0,1:T(4,128)(2,1)}, u32[]{:S(2)}) copy-start(bf16[2048,4]{0,1:T(4,128)(2,1)} %param.26) | copy-start | bytes 49156
  30.4 4.3 %copy-start.10 = (bf16[2048,4]{0,1:T(4,128)(2,1)S(1)}, bf16[2048,4]{0,1:T(4,128)(2,1)}, u32[]{:S(2)}) copy-start(bf16[2048,4]{0,1:T(4,128)(2,1)} %param.27) | copy-start | bytes 49156
  30.4 22.6 %all-to-all-start = ((bf16[4,1,96,2048]{3,2,1,0:T(8,128)(2,1)}), bf16[4,1,96,2048]{3,2,1,0:T(8,128)(2,1)S(1)}, u32[]{:S(2)}, u32[]{:S(2)}) async-start(bf16[4,1,96,2048]{3,2,1,0:T(8,128)(2,1)} %bitcast.11), calls=%async_computation.1 | async-start | bytes 3145728 | tf_op jit(solution)/shard_map/all_to_all | solution.py:119
  164.1 42.9 %copy-start.5 = (f32[2048]{0:T(1024)S(1)}, f32[2048]{0:T(1024)}, u32[]{:S(2)}) copy-start(f32[2048]{0:T(1024)} %param.22) | copy-start | bytes 24580
  164.1 44.9 %all-to-all-start.1 = ((bf16[4,1,96,2048]{3,2,1,0:T(8,128)(2,1)}), bf16[4,1,96,2048]{3,2,1,0:T(8,128)(2,1)S(1)}, u32[]{:S(2)}, u32[]{:S(2)}) async-start(bf16[4,1,96,2048]{3,2,1,0:T(8,128)(2,1)} %fusion.9), calls=%async_computation.2 | async-start | bytes 3145728 | tf_op jit(solution)/shard_map/all_to_all | solution.py:127
  211.1 4.3 %copy-start.6 = (f32[2048]{0:T(1024)S(1)}, f32[2048]{0:T(1024)}, u32[]{:S(2)}) copy-start(f32[2048]{0:T(1024)} %param.25) | copy-start | bytes 24580
Sparse Core Ops, SparseCore 0:
  9.6 50.5 all-gather.5
  61.7 45.9 all-gather.3
  109.4 45.9 all-gather.7
  157.6 48.1 reduce-scatter.1
where the time goes:
time: 223 us
  waiting for transfers between devices  155 us (70%)
  matrix products  20.5 us (9%)
  starting transfers between devices  16.2 us (7%)
  between operations  14.2 us (6%)
  other arithmetic  11.3 us (5%)
  local copies, waits for them, and re-layouts  6.18 us (3%)
    all_gather x1, waiting for transfers between devices, per_device(): down_piece = lax.all_gather(down_weight, 'tp', axis=2, tiled=True)  47.6 us
    all_gather x1, waiting for transfers between devices, per_device(): gate_piece = lax.all_gather(gate_weight, 'tp', axis=2, tiled=True)  42.5 us
    reduce_scatter x1, waiting for transfers between devices, per_device(): lax.psum_scatter(jnp.dot(attention, out_weight, preferred_element_type=jn...  37.6 us
    all_to_all x1, waiting for transfers between devices, per_device(): lax.all_to_all(outgoing, 'ep', split_axis=0, concat_axis=0, tiled=True)  17.6 us
    dot_general x1, matrix products, per_device(): jnp.einsum('sxcf,xdf->sxcd', hidden, down_piece, preferred_element_type=j...  8.63 us
    ppermute x2, starting transfers between devices, shifted(): return lax.ppermute(block, axis, route)  8.27 us
    all_gather x1, waiting for transfers between devices, per_device(): up_piece = lax.all_gather(up_weight, 'tp', axis=2, tiled=True)  7.09 us
    dot_general x1, matrix products, per_device(): jnp.einsum('sxcd,xdf->sxcf', arrived, up_piece, preferred_element_type=jn...  5.13 us
  transfers between devices with their start and end apart: 8, of which 5 were waited for; matrix products, arithmetic and copies ran while one was open for 13% of the time, Pallas kernels for 0%

commit v1 on v0

--- a/solution.py
+++ b/solution.py
@@ -9,6 +9,20 @@
 KV_HEADS = 4
 WINDOW = 128
 eps = 1e-06
+
+
+def work_both_ways(array, axis, dim, make, out_dim):
+    ways, here, lap = (lax.axis_size(axis), lax.axis_index(axis), array.shape[dim])
+    earlier, later = ([], [])
+    going_up = going_down = array
+    for far in range(ways // 2 + 1):
+        earlier.append(make(going_up, (here - far) % ways * lap))
+        if 0 < far < ways - ways // 2:
+            later.append(make(going_down, (here + far) % ways * lap))
+        going_up = lax.ppermute(going_up, axis, [(d, (d + 1) % ways) for d in range(ways)])
+        going_down = lax.ppermute(going_down, axis, [(d, (d - 1) % ways) for d in range(ways)])
+    line = jnp.concatenate([*earlier[::-1], *later], axis=out_dim)
+    return jnp.roll(line, (here - ways // 2) * earlier[0].shape[out_dim], axis=out_dim)
 
 
 def shifted(block, axis, distance):
@@ -117,10 +131,17 @@
     local_experts = gate_weight.shape[0]
     outgoing = outgoing.reshape(lax.axis_size("ep"), local_experts, capacity, normed.shape[1])
     arrived = lax.all_to_all(outgoing, "ep", split_axis=0, concat_axis=0, tiled=True)
-    gate_piece = lax.all_gather(gate_weight, "tp", axis=2, tiled=True)
     up_piece = lax.all_gather(up_weight, "tp", axis=2, tiled=True)
     down_piece = lax.all_gather(down_weight, "tp", axis=2, tiled=True)
-    gate = jnp.einsum("sxcd,xdf->sxcf", arrived, gate_piece, preferred_element_type=jnp.float32)
+    gate = work_both_ways(
+        gate_weight,
+        "tp",
+        2,
+        lambda part, offset: jnp.einsum(
+            "sxcd,xdf->sxcf", arrived, part, preferred_element_type=jnp.float32
+        ),
+        3,
+    )
     up = jnp.einsum("sxcd,xdf->sxcf", arrived, up_piece, preferred_element_type=jnp.float32)
     hidden = (jax.nn.silu(gate) * up).astype(jnp.bfloat16)
     results = jnp.einsum("sxcf,xdf->sxcd", hidden, down_piece, preferred_element_type=jnp.float32)

time: 223 us -> 208 us (0.933)
  waiting for transfers between devices: 155 us -> 109 us
  starting transfers between devices: 16.2 us -> 28.4 us
  matrix products: 20.5 us -> 31.8 us
  local copies, waits for them, and re-layouts: 6.18 us -> 12.2 us
    ppermute x0 -> x7, waiting for transfers between devices: none -> 71.4 us  [the longest x4 69.1 us: work_both_ways(): lax.ppermute(going_up, axis, [(d, (d + 1) % ways) for d in range(ways)])]
    all_gather x1, waiting for transfers between devices: 47.6 us -> 0.01 us  [per_device(): down_piece = lax.all_gather(down_weight, 'tp', axis=2, tiled=True)]
    all_gather x1 -> x0, waiting for transfers between devices: 42.5 us -> none  [per_device(): gate_piece = lax.all_gather(gate_weight, 'tp', axis=2, tiled=True)]
    all_to_all x1, waiting for transfers between devices: 17.6 us -> 0.01 us  [per_device(): lax.all_to_all(outgoing, 'ep', split_axis=0, concat_axis=0, tiled=True)]
    dot_general x1 -> x8, matrix products: 5.13 us -> 16.5 us  [per_device(): jnp.einsum('sxcd,xdf->sxcf', arrived, part, preferred_element_type=jnp.fl...]
    ppermute x0 -> x7, starting transfers between devices: none -> 10.8 us  [the longest x3 10.8 us: work_both_ways(): lax.ppermute(going_down, axis, [(d, (d - 1) % ways) for d in range(ways)])]
    all_gather x1, waiting for transfers between devices: 7.09 us -> 0.01 us  [per_device(): up_piece = lax.all_gather(up_weight, 'tp', axis=2, tiled=True)]
    unnamed x25 -> x34, local copies, waits for them, and re-layouts: 1.09 us -> 6.41 us
  transfers between devices with their start and end apart: 8 -> 14, of which waited for: 5 -> 6; matrix products, arithmetic and copies ran while one was open for 13% -> 23% of each run, Pallas kernels for 0% -> 0%
where the time goes in v1:
time: 208 us; the launch traced here: 207 us
  waiting for transfers between devices  109 us (52%)
  matrix products  31.8 us (15%)
  starting transfers between devices  28.4 us (14%)
  between operations  14.1 us (7%)
  local copies, waits for them, and re-layouts  12.2 us (6%)
  other arithmetic  11.3 us (5%)
    ppermute x4, waiting for transfers between devices, work_both_ways(): lax.ppermute(going_up, axis, [(d, (d + 1) % ways) for d in range(ways)])  69.1 us
    reduce_scatter x1, waiting for transfers between devices, per_device(): lax.psum_scatter(jnp.dot(attention, out_weight, preferred_element_type=jn...  36.6 us
    dot_general x8, matrix products, per_device(): jnp.einsum('sxcd,xdf->sxcf', arrived, part, preferred_element_type=jnp.fl...  16.5 us
    ppermute x3, starting transfers between devices, work_both_ways(): lax.ppermute(going_down, axis, [(d, (d - 1) % ways) for d in range(ways)])  10.8 us
    dot_general x1, matrix products, per_device(): jnp.einsum('sxcf,xdf->sxcd', hidden, down_piece, preferred_element_type=j...  8.55 us
    ppermute x2, starting transfers between devices, shifted(): return lax.ppermute(block, axis, route)  8.27 us
    unnamed x34, local copies, waits for them, and re-layouts  6.41 us
    all_to_all x1, starting transfers between devices, per_device(): lax.all_to_all(results.astype(jnp.bfloat16), 'ep', split_axis=0, concat_a...  5.39 us
  transfers between devices with their start and end apart: 14, of which 6 were waited for; matrix products, arithmetic and copies ran while one was open for 23% of the time, Pallas kernels for 0%

profile of v1, /device:TPU:0, one launch (start us, length us, event | category | flops | bytes accessed | tf_op | source)
XLA Modules:
  0.0 207.2 jit_solution(10247556295352911677)
XLA Ops:
  8.8 1.2 constant_dynamic-slice_fusion
  10.1 4.9 %collective-permute-start.1 = (bf16[128,64]{0,1:T(8,128)(2,1)S(1)}, bf16[128,64]{0,1:T(8,128)(2,1)S(1)}, u32[]{:S(2)}, u32[]{:S(2)}) collective-permute-start(bf16[128,64]{0,1:T(8,128)(2,1)S(1)} %slice.36), channel_id=1, source_target_pairs={{0,8},{8,16},{16,24},{1,9},{9,17},{17,25},{2,10},{10,18},{18,26},{... | collective-permute-start | bytes 49160 | tf_op jit(solution)/shard_map/ppermute | solution.py:31
  15.2 3.4 %collective-permute-start = (bf16[128,64]{0,1:T(8,128)(2,1)S(1)}, bf16[128,64]{0,1:T(8,128)(2,1)S(1)}, u32[]{:S(2)}, u32[]{:S(2)}) collective-permute-start(bf16[128,64]{0,1:T(8,128)(2,1)S(1)} %slice.34), channel_id=1, source_target_pairs={{0,8},{8,16},{16,24},{1,9},{9,17},{17,25},{2,10},{10,18},{18,26},{... | collective-permute-start | bytes 49160 | tf_op jit(solution)/shard_map/ppermute | solution.py:31
  21.4 3.2 %convolution_convert_fusion = bf16[1024,2048]{1,0:T(8,128)(2,1)} fusion(bf16[128,2048]{1,0:T(8,128)(2,1)S(1)} %copy-done, bf16[16,8,8,128]{3,2,1,0:T(8,128)(2,1)S(1)} %bitcast.273), kind=kOutput, calls=%fused_computation.5 | convolution fusion | flops 538968064 | bytes 4980736 | tf_op jit(solution)/shard_map/dot_general | solution.py:100
  24.7 1.0 copy-done.2
  25.7 3.5 %collective-permute-start.6 = (bf16[1,2048,128]{2,1,0:T(8,128)(2,1)S(1)}, bf16[1,2048,128]{2,1,0:T(8,128)(2,1)}, u32[]{:S(2)}, u32[]{:S(2)}) collective-permute-start(bf16[1,2048,128]{2,1,0:T(8,128)(2,1)S(1)} %copy-done.2), channel_id=1, source_target_pairs={{0,7},{1,0},{2,1},{3,2},{4,3},{5,4},{6,5},{7,6},{8,15},{9,8},{10,9... | collective-permute-start | bytes 1572872 | tf_op jit(solution)/shard_map/ppermute | solution.py:23
  29.6 1.2 reduce-window.6
  31.7 20.8 %collective-permute-done.2 = bf16[1,2048,128]{2,1,0:T(8,128)(2,1)} collective-permute-done((bf16[1,2048,128]{2,1,0:T(8,128)(2,1)S(1)}, bf16[1,2048,128]{2,1,0:T(8,128)(2,1)}, u32[]{:S(2)}, u32[]{:S(2)}) %collective-permute-start.2) | collective-permute-done | bytes 524320 | tf_op jit(solution)/shard_map/ppermute | solution.py:22
  52.6 1.8 convolution_convert_fusion.1
  54.4 3.9 %all-to-all-start = ((bf16[4,1,96,2048]{3,2,1,0:T(8,128)(2,1)}), bf16[4,1,96,2048]{3,2,1,0:T(8,128)(2,1)S(1)}, u32[]{:S(2)}, u32[]{:S(2)}) async-start(bf16[4,1,96,2048]{3,2,1,0:T(8,128)(2,1)} %bitcast.272), calls=%async_computation.1 | async-start | bytes 3145728 | tf_op jit(solution)/shard_map/all_to_all | solution.py:133
  58.6 16.0 %collective-permute-done.3 = bf16[1,2048,128]{2,1,0:T(8,128)(2,1)} collective-permute-done((bf16[1,2048,128]{2,1,0:T(8,128)(2,1)}, bf16[1,2048,128]{2,1,0:T(8,128)(2,1)}, u32[]{:S(2)}, u32[]{:S(2)}) %collective-permute-start.3) | collective-permute-done | bytes 524320 | tf_op jit(solution)/shard_map/ppermute | solution.py:22
  75.0 3.6 %collective-permute-start.7 = (bf16[1,2048,128]{2,1,0:T(8,128)(2,1)}, bf16[1,2048,128]{2,1,0:T(8,128)(2,1)S(1)}, u32[]{:S(2)}, u32[]{:S(2)}) collective-permute-start(bf16[1,2048,128]{2,1,0:T(8,128)(2,1)} %collective-permute-done.6), channel_id=1, source_target_pairs={{0,7},{1,0},{2,1},{3,2},{4,3},{5,4},{6,5},{7,6},{8,15},{9,8},{10,9... | collective-permute-start | bytes 1572872 | tf_op jit(solution)/shard_map/ppermute | solution.py:23
  78.6 11.7 %collective-permute-done.4 = bf16[1,2048,128]{2,1,0:T(8,128)(2,1)} collective-permute-done((bf16[1,2048,128]{2,1,0:T(8,128)(2,1)}, bf16[1,2048,128]{2,1,0:T(8,128)(2,1)}, u32[]{:S(2)}, u32[]{:S(2)}) %collective-permute-start.4) | collective-permute-done | bytes 524320 | tf_op jit(solution)/shard_map/ppermute | solution.py:22
  90.7 2.3 %collective-permute-done.7 = bf16[1,2048,128]{2,1,0:T(8,128)(2,1)S(1)} collective-permute-done((bf16[1,2048,128]{2,1,0:T(8,128)(2,1)}, bf16[1,2048,128]{2,1,0:T(8,128)(2,1)S(1)}, u32[]{:S(2)}, u32[]{:S(2)}) %collective-permute-start.7) | collective-permute-done | bytes 524320 | tf_op jit(solution)/shard_map/ppermute | solution.py:23
  93.0 3.7 %collective-permute-start.8 = (bf16[1,2048,128]{2,1,0:T(8,128)(2,1)S(1)}, bf16[1,2048,128]{2,1,0:T(8,128)(2,1)}, u32[]{:S(2)}, u32[]{:S(2)}) collective-permute-start(bf16[1,2048,128]{2,1,0:T(8,128)(2,1)S(1)} %collective-permute-done.7), channel_id=1, source_target_pairs={{0,7},{1,0},{2,1},{3,2},{4,3},{5,4},{6,5},{7,6},{8,15},{9,8},{10,9... | collective-permute-start | bytes 1572872 | tf_op jit(solution)/shard_map/ppermute | solution.py:23
  96.6 20.6 %collective-permute-done.5 = bf16[1,2048,128]{2,1,0:T(8,128)(2,1)} collective-permute-done((bf16[1,2048,128]{2,1,0:T(8,128)(2,1)}, bf16[1,2048,128]{2,1,0:T(8,128)(2,1)}, u32[]{:S(2)}, u32[]{:S(2)}) %collective-permute-start.5) | collective-permute-done | bytes 524320 | tf_op jit(solution)/shard_map/ppermute | solution.py:22
  117.2 2.3 %constant_dynamic-update-slice_fusion.15 = (f32[4,1,96,2048]{3,2,0,1:T(8,128)}, f32[4,1,96,128]{3,2,0,1:T(8,128)S(1)}) fusion(bf16[1,2048,128]{2,1,0:T(8,128)(2,1)} %collective-permute-done.5, bf16[4,1,96,2048]{3,2,1,0:T(8,128)(2,1)S(1)} %all-to-all-done), kind=kOutput, calls=%fused_computation.110 | convolution fusion | flops 201326592 | bytes 2490368 | tf_op jit(solution)/shard_map/sxcd,xdf->sxcf/dot_general | solution.py:140
  119.6 2.3 %constant_dynamic-update-slice_fusion.14 = (f32[4,1,96,2048]{3,2,0,1:T(8,128)}, f32[4,1,96,128]{3,2,0,1:T(8,128)S(1)}) fusion(f32[4,1,96,2048]{3,2,0,1:T(8,128)} %get-tuple-element.8, bf16[1,2048,128]{2,1,0:T(8,128)(2,1)} %collective-permute-done.4, bf16[4,1,96,2048]{3,2,1,0:T(8,128)(2,1)S(1)} %all-to-all-done), kind=kOutput, calls=%fused_computation.109 | convolution fusion | flops 201326592 | bytes 2490368 | tf_op jit(solution)/shard_map/sxcd,xdf->sxcf/dot_general | solution.py:140
  121.9 2.3 %constant_dynamic-update-slice_fusion.13 = (f32[4,1,96,2048]{3,2,0,1:T(8,128)}, f32[4,1,96,128]{3,2,0,1:T(8,128)S(1)}) fusion(f32[4,1,96,2048]{3,2,0,1:T(8,128)} %get-tuple-element.10, bf16[1,2048,128]{2,1,0:T(8,128)(2,1)} %collective-permute-done.3, bf16[4,1,96,2048]{3,2,1,0:T(8,128)(2,1)S(1)} %all-to-all-done), kind=kOutput, calls=%fused_computation.108 | convolution fusion | flops 201326592 | bytes 2490368 | tf_op jit(solution)/shard_map/sxcd,xdf->sxcf/dot_general | solution.py:140
  124.2 2.3 %constant_dynamic-update-slice_fusion.12 = (f32[4,1,96,2048]{3,2,0,1:T(8,128)}, f32[4,1,96,128]{3,2,0,1:T(8,128)S(1)}) fusion(f32[4,1,96,2048]{3,2,0,1:T(8,128)} %get-tuple-element.12, bf16[1,2048,128]{2,1,0:T(8,128)(2,1)} %collective-permute-done.2, bf16[4,1,96,2048]{3,2,1,0:T(8,128)(2,1)S(1)} %all-to-all-done), kind=kOutput, calls=%fused_computation.107 | convolution fusion | flops 201326592 | bytes 2490368 | tf_op jit(solution)/shard_map/sxcd,xdf->sxcf/dot_general | solution.py:140
  126.5 1.3 constant_dynamic-update-slice_fusion.11
  127.8 2.3 %constant_dynamic-update-slice_fusion.10 = (f32[4,1,96,2048]{3,2,0,1:T(8,128)}, f32[4,1,96,128]{3,2,0,1:T(8,128)S(1)}) fusion(f32[4,1,96,2048]{3,2,0,1:T(8,128)} %get-tuple-element.16, bf16[1,2048,128]{2,1,0:T(8,128)(2,1)} %collective-permute-done.6, bf16[4,1,96,2048]{3,2,1,0:T(8,128)(2,1)S(1)} %all-to-all-done), kind=kOutput, calls=%fused_computation.105 | convolution fusion | flops 201326592 | bytes 2490368 | tf_op jit(solution)/shard_map/sxcd,xdf->sxcf/dot_general | solution.py:140
  130.1 1.3 constant_dynamic-update-slice_fusion.9
  131.4 2.4 %constant_dynamic-update-slice_fusion.8 = (f32[4,1,96,2048]{3,2,0,1:T(8,128)}, f32[4,1,96,128]{3,2,0,1:T(8,128)S(1)}) fusion(f32[4,1,96,2048]{3,2,0,1:T(8,128)} %get-tuple-element.20, bf16[1,2048,128]{2,1,0:T(8,128)(2,1)} %collective-permute-done.8, bf16[4,1,96,2048]{3,2,1,0:T(8,128)(2,1)S(1)} %all-to-all-done), kind=kOutput, calls=%fused_computation.103 | convolution fusion | flops 201326592 | bytes 2490368 | tf_op jit(solution)/shard_map/sxcd,xdf->sxcf/dot_general | solution.py:140
  139.4 8.6 %fusion.7 = bf16[4,1,96,2048]{3,2,1,0:T(8,128)(2,1)} fusion(bf16[1,2048,1024]{2,1,0:T(8,128)(2,1)} %all-gather.5.cloned.1.call-done, bf16[1,2048,1024]{2,1,0:T(8,128)(2,1)} %all-gather.3.cloned.1.call-done, bf16[4,1,96,2048]{3,2,1,0:T(8,128)(2,1)S(1)} %all-to-all-done, f32[4,1,96,2048]{3,2,0,1:T(8,128)} %constant_dynamic-update-slice_fusion, s32[]{:T(128)S(6)} %select_n.64), kind=kOutput, calls=%fused_computation.8 | convolution fusion | flops 3224371200 | bytes 13107204 | tf_op jit(solution)/shard_map/sxcf,xdf->sxcd/dot_general | solution.py:147
  148.0 5.4 %all-to-all-start.1 = ((bf16[4,1,96,2048]{3,2,1,0:T(8,128)(2,1)}), bf16[4,1,96,2048]{3,2,1,0:T(8,128)(2,1)S(1)}, u32[]{:S(2)}, u32[]{:S(2)}) async-start(bf16[4,1,96,2048]{3,2,1,0:T(8,128)(2,1)} %fusion.7), calls=%async_computation.2 | async-start | bytes 3145728 | tf_op jit(solution)/shard_map/all_to_all | solution.py:148
  153.5 36.6 %reduce-scatter.2.cloned.1.call-done = bf16[128,2048]{1,0:T(8,128)(2,1)} async-done(((bf16[1024,2048]{1,0:T(8,128)(2,1)}), bf16[128,2048]{1,0:T(8,128)(2,1)}) %reduce-scatter.2.cloned.1.call-update) | async-done | bytes 524304 | tf_op jit(solution)/shard_map/reduce_scatter | solution.py:99
  190.1 1.2 fusion.64
  191.3 2.0 fusion.66
  193.4 1.4 gather_fusion
  195.5 4.1 %multiply_reduce_fusion = f32[128,2048]{1,0:T(8,128)S(1)} fusion(bf16[128,2,2048]{2,1,0:T(2,128)(2,1)S(1)} %gather.7, pred[128,2]{1,0:T(8,128)(4,1)S(1)} %copy.102, f32[128,2]{1,0:T(8,128)S(1)} %copy.96), kind=kLoop, calls=%fused_computation.11 | loop fusion | flops 1835008 | bytes 2098432 | tf_op jit(solution)/shard_map/reduce_sum | solution.py:155
  199.7 1.0 multiply_convert_fusion
  (107 shorter events, 13.6 us)
Async XLA Ops:
  7.2 14.3 %copy-start = (bf16[128,2048]{1,0:T(8,128)(2,1)S(1)}, bf16[128,2048]{1,0:T(8,128)(2,1)}, u32[]{:S(2)}) copy-start(bf16[128,2048]{1,0:T(8,128)(2,1)} %param.21) | copy-start | bytes 1572868
  7.2 12.0 %copy-start.9 = (f32[2]{0:T(128)S(1)}, f32[2]{0:T(128)}, u32[]{:S(2)}) copy-start(f32[2]{0:T(128)} %param.19) | copy-start | bytes 28
  7.2 132.2 %all-gather.3.cloned.1.call-start = ((), (), s32[]{:S(2)}) async-start(), calls=%async_computation.4 | async-start | bytes 4718592 | tf_op jit(solution)/shard_map/all_gather | solution.py:134
  7.9 11.4 %copy-start.3 = (bf16[1024,128]{1,0:T(8,128)(2,1)S(1)}, bf16[1024,128]{1,0:T(8,128)(2,1)}, u32[]{:S(2)}) copy-start(bf16[1024,128]{1,0:T(8,128)(2,1)} %param.16) | copy-start | bytes 786436
  7.9 131.5 %all-gather.5.cloned.1.call-start = ((), (), s32[]{:S(2)}) async-start(), calls=%async_computation.5 | async-start | bytes 4718592 | tf_op jit(solution)/shard_map/all_gather | solution.py:135
  8.7 181.4 %reduce-scatter.2.cloned.1.call-start = ((), (), s32[]{:S(2)}) async-start(), calls=%async_computation.3 | async-start | bytes 4718592 | tf_op jit(solution)/shard_map/reduce_scatter | solution.py:99
  10.1 9.4 %collective-permute-start.1 = (bf16[128,64]{0,1:T(8,128)(2,1)S(1)}, bf16[128,64]{0,1:T(8,128)(2,1)S(1)}, u32[]{:S(2)}, u32[]{:S(2)}) collective-permute-start(bf16[128,64]{0,1:T(8,128)(2,1)S(1)} %slice.36), channel_id=1, source_target_pairs={{0,8},{8,16},{16,24},{1,9},{9,17},{17,25},{2,10},{10,18},{18,26},{... | collective-permute-start | bytes 49160 | tf_op jit(solution)/shard_map/ppermute | solution.py:31
  15.2 5.6 %collective-permute-start = (bf16[128,64]{0,1:T(8,128)(2,1)S(1)}, bf16[128,64]{0,1:T(8,128)(2,1)S(1)}, u32[]{:S(2)}, u32[]{:S(2)}) collective-permute-start(bf16[128,64]{0,1:T(8,128)(2,1)S(1)} %slice.34), channel_id=1, source_target_pairs={{0,8},{8,16},{16,24},{1,9},{9,17},{17,25},{2,10},{10,18},{18,26},{... | collective-permute-start | bytes 49160 | tf_op jit(solution)/shard_map/ppermute | solution.py:31
  19.6 0.7 copy-start.8
  24.6 1.0 copy-start.2
  24.6 4.6 %copy-start.4 = (s32[128,2]{0,1:T(2,128)S(1)}, s32[128,2]{0,1:T(2,128)}, u32[]{:S(2)}) copy-start(s32[128,2]{0,1:T(2,128)} %param.28) | copy-start | bytes 3076
  24.6 6.8 %copy-start.1 = (bf16[128,2048]{1,0:T(8,128)(2,1)S(1)}, bf16[128,2048]{1,0:T(8,128)(2,1)}, u32[]{:S(2)}) copy-start(bf16[128,2048]{1,0:T(8,128)(2,1)} %param.23) | copy-start | bytes 1572868
  24.7 27.9 %copy-start.5 = (f32[2048]{0:T(1024)S(1)}, f32[2048]{0:T(1024)}, u32[]{:S(2)}) copy-start(f32[2048]{0:T(1024)} %param.24) | copy-start | bytes 24580
  25.7 26.8 %collective-permute-start.2 = (bf16[1,2048,128]{2,1,0:T(8,128)(2,1)S(1)}, bf16[1,2048,128]{2,1,0:T(8,128)(2,1)}, u32[]{:S(2)}, u32[]{:S(2)}) collective-permute-start(bf16[1,2048,128]{2,1,0:T(8,128)(2,1)S(1)} %copy-done.2), channel_id=1, source_target_pairs={{0,1},{1,2},{2,3},{3,4},{4,5},{5,6},{6,7},{7,0},{8,9},{9,10},{10,1... | collective-permute-start | bytes 1572872 | tf_op jit(solution)/shard_map/ppermute | solution.py:22
  25.7 49.3 %collective-permute-start.6 = (bf16[1,2048,128]{2,1,0:T(8,128)(2,1)S(1)}, bf16[1,2048,128]{2,1,0:T(8,128)(2,1)}, u32[]{:S(2)}, u32[]{:S(2)}) collective-permute-start(bf16[1,2048,128]{2,1,0:T(8,128)(2,1)S(1)} %copy-done.2), channel_id=1, source_target_pairs={{0,7},{1,0},{2,1},{3,2},{4,3},{5,4},{6,5},{7,6},{8,15},{9,8},{10,9... | collective-permute-start | bytes 1572872 | tf_op jit(solution)/shard_map/ppermute | solution.py:23
  52.5 22.1 %collective-permute-start.3 = (bf16[1,2048,128]{2,1,0:T(8,128)(2,1)}, bf16[1,2048,128]{2,1,0:T(8,128)(2,1)}, u32[]{:S(2)}, u32[]{:S(2)}) collective-permute-start(bf16[1,2048,128]{2,1,0:T(8,128)(2,1)} %collective-permute-done.2), channel_id=1, source_target_pairs={{0,1},{1,2},{2,3},{3,4},{4,5},{5,6},{6,7},{7,0},{8,9},{9,10},{10,1... | collective-permute-start | bytes 1572872 | tf_op jit(solution)/shard_map/ppermute | solution.py:22
  54.4 3.9 %copy-start.10 = (bf16[2048,4]{0,1:T(4,128)(2,1)S(1)}, bf16[2048,4]{0,1:T(4,128)(2,1)}, u32[]{:S(2)}) copy-start(bf16[2048,4]{0,1:T(4,128)(2,1)} %param.26) | copy-start | bytes 49156
  54.4 20.3 %copy-start.11 = (bf16[2048,4]{0,1:T(4,128)(2,1)S(1)}, bf16[2048,4]{0,1:T(4,128)(2,1)}, u32[]{:S(2)}) copy-start(bf16[2048,4]{0,1:T(4,128)(2,1)} %param.27) | copy-start | bytes 49156
  54.4 42.2 %all-to-all-start = ((bf16[4,1,96,2048]{3,2,1,0:T(8,128)(2,1)}), bf16[4,1,96,2048]{3,2,1,0:T(8,128)(2,1)S(1)}, u32[]{:S(2)}, u32[]{:S(2)}) async-start(bf16[4,1,96,2048]{3,2,1,0:T(8,128)(2,1)} %bitcast.272), calls=%async_computation.1 | async-start | bytes 3145728 | tf_op jit(solution)/shard_map/all_to_all | solution.py:133
  74.6 15.6 %collective-permute-start.4 = (bf16[1,2048,128]{2,1,0:T(8,128)(2,1)}, bf16[1,2048,128]{2,1,0:T(8,128)(2,1)}, u32[]{:S(2)}, u32[]{:S(2)}) collective-permute-start(bf16[1,2048,128]{2,1,0:T(8,128)(2,1)} %collective-permute-done.3), channel_id=1, source_target_pairs={{0,1},{1,2},{2,3},{3,4},{4,5},{5,6},{6,7},{7,0},{8,9},{9,10},{10,1... | collective-permute-start | bytes 1572872 | tf_op jit(solution)/shard_map/ppermute | solution.py:22
  75.0 18.0 %collective-permute-start.7 = (bf16[1,2048,128]{2,1,0:T(8,128)(2,1)}, bf16[1,2048,128]{2,1,0:T(8,128)(2,1)S(1)}, u32[]{:S(2)}, u32[]{:S(2)}) collective-permute-start(bf16[1,2048,128]{2,1,0:T(8,128)(2,1)} %collective-permute-done.6), channel_id=1, source_target_pairs={{0,7},{1,0},{2,1},{3,2},{4,3},{5,4},{6,5},{7,6},{8,15},{9,8},{10,9... | collective-permute-start | bytes 1572872 | tf_op jit(solution)/shard_map/ppermute | solution.py:23
  90.2 27.0 %collective-permute-start.5 = (bf16[1,2048,128]{2,1,0:T(8,128)(2,1)}, bf16[1,2048,128]{2,1,0:T(8,128)(2,1)}, u32[]{:S(2)}, u32[]{:S(2)}) collective-permute-start(bf16[1,2048,128]{2,1,0:T(8,128)(2,1)} %collective-permute-done.4), channel_id=1, source_target_pairs={{0,1},{1,2},{2,3},{3,4},{4,5},{5,6},{6,7},{7,0},{8,9},{9,10},{10,1... | collective-permute-start | bytes 1572872 | tf_op jit(solution)/shard_map/ppermute | solution.py:22
  93.0 38.4 %collective-permute-start.8 = (bf16[1,2048,128]{2,1,0:T(8,128)(2,1)S(1)}, bf16[1,2048,128]{2,1,0:T(8,128)(2,1)}, u32[]{:S(2)}, u32[]{:S(2)}) collective-permute-start(bf16[1,2048,128]{2,1,0:T(8,128)(2,1)S(1)} %collective-permute-done.7), channel_id=1, source_target_pairs={{0,7},{1,0},{2,1},{3,2},{4,3},{5,4},{6,5},{7,6},{8,15},{9,8},{10,9... | collective-permute-start | bytes 1572872 | tf_op jit(solution)/shard_map/ppermute | solution.py:23
  148.0 43.4 %copy-start.6 = (f32[2048]{0:T(1024)S(1)}, f32[2048]{0:T(1024)}, u32[]{:S(2)}) copy-start(f32[2048]{0:T(1024)} %param.22) | copy-start | bytes 24580
  148.0 45.4 %all-to-all-start.1 = ((bf16[4,1,96,2048]{3,2,1,0:T(8,128)(2,1)}), bf16[4,1,96,2048]{3,2,1,0:T(8,128)(2,1)S(1)}, u32[]{:S(2)}, u32[]{:S(2)}) async-start(bf16[4,1,96,2048]{3,2,1,0:T(8,128)(2,1)} %fusion.7), calls=%async_computation.2 | async-start | bytes 3145728 | tf_op jit(solution)/shard_map/all_to_all | solution.py:148
  195.5 4.3 %copy-start.7 = (f32[2048]{0:T(1024)S(1)}, f32[2048]{0:T(1024)}, u32[]{:S(2)}) copy-start(f32[2048]{0:T(1024)} %param.25) | copy-start | bytes 24580
Sparse Core Ops, SparseCore 0:
  9.6 67.3 all-gather.2
  78.6 59.6 all-gather.4
  140.6 49.4 reduce-scatter.1
